TPU v7x, 32 devices: a whole 2x2x4 slice. The times are simulated.
32 devices in a mesh: kv: 8 (over z, core), tp: 4 (over y, x).
Axes of the slice: x: 2, y: 2, z: 4, core: 2. Of those that a mesh axis runs over, the one named last changes fastest.
Arguments:
- tokens: bfloat16 [16, 2048], P(None, 'kv'), may hold values from -8 to 8
- lengths: int32 [16], replicated, may hold values from 1 to 3072, 12288 in all
- latent_cache: bfloat16 [16, 3072, 256], P(None, ('kv', 'tp')), may hold values from -10 to 10
- rope_cache: bfloat16 [16, 3072, 32], P(None, ('kv', 'tp')), may hold values from -2000 to 2000
- gain_in: bfloat16 [2048], P('kv'), may hold values from 0.099609375 to 1.8984375
- w_down_q: bfloat16 [2048, 512], P('kv'), may hold values from -0.125 to 0.125
- w_down_kv: bfloat16 [2048, 256], P('kv'), may hold values from -0.125 to 0.125
- w_rope_key: bfloat16 [2048, 32], P('kv'), may hold values from -0.125 to 0.125
- gain_q: bfloat16 [512], replicated, may hold values from 0.099609375 to 1.8984375
- w_up_qn: bfloat16 [512, 16, 64], replicated, may hold values from -0.25 to 0.25
- w_up_qr: bfloat16 [512, 16, 32], replicated, may hold values from -0.25 to 0.25
- gain_kv: bfloat16 [256], replicated, may hold values from 0.099609375 to 1.8984375
- w_key_up: bfloat16 [256, 16, 64], replicated, may hold values from -0.375 to 0.375
- w_value_up: bfloat16 [256, 16, 64], replicated, may hold values from -0.375 to 0.375
- w_attn_out: bfloat16 [16, 64, 2048], P('tp', None, 'kv'), may hold values from -0.1875 to 0.1875
- gain_mid: bfloat16 [2048], P('kv'), may hold values from 0.099609375 to 1.8984375
- w_ff_in: bfloat16 [2048, 8192], P('kv', 'tp'), may hold values from -0.125 to 0.125
- w_ff_out: bfloat16 [8192, 2048], P('tp', 'kv'), may hold values from -0.0625 to 0.0625
Outputs:
- mixed: bfloat16 [16, 2048], P(None, 'kv')
- new_latent: bfloat16 [16, 256], replicated
- new_rope_key: bfloat16 [16, 32], replicated
Inputs may be any that keep to these rules, and one draw needn't show every extreme that they name: `lengths`: each sequence's live cache positions; one sequence fills the whole cache.
All inputs are finite; a program needn't handle non-finite values.
Results may differ from a plain program's by a relative error of at most 0.012.
Values sent between devices are 32-bit elements; how exact they have to be, the bound alone decides.
No kernel may reach another device: no remote copies, remote signals or barrier semaphores. Data moves between devices by JAX's collectives and lax.ppermute only.
A program may use at most 64 MiB of HBM per device.

v0:
```python
import jax
import jax.numpy as jnp
from jax import lax
from jax.sharding import PartitionSpec as P

D = 2048
NOPE = 64
ROPE = 32
EPS = 1e-06


def combined_all(part, axis, combine):
    gathered = jax.tree.map(lambda a: lax.all_gather(a, axis), part)

    def take(source):
        return jax.tree.map(lambda a: lax.dynamic_index_in_dim(a, source, 0, False), gathered)

    return lax.fori_loop(
        1, lax.axis_size(axis), lambda source, state: combine(state, take(source)), take(0)
    )


def rotate(values, positions):
    half = values.shape[-1] // 2
    inverse = 10000.0 ** (-jnp.arange(half, dtype=jnp.float32) / half)
    angle = positions.astype(jnp.float32)[:, None, None] * inverse[None, None, :]
    first = values[..., :half]
    second = values[..., half:]
    return jnp.concatenate(
        [
            first * jnp.cos(angle) - second * jnp.sin(angle),
            second * jnp.cos(angle) + first * jnp.sin(angle),
        ],
        axis=-1,
    )


def rms_scaled(values, gain):
    return (
        values
        * lax.rsqrt(jnp.mean(values * values, axis=-1, keepdims=True) + EPS)
        * gain.astype(jnp.float32)
    )


def combine(earlier, later):
    top_a, total_a, acc_a = earlier
    top_b, total_b, acc_b = later
    top = jnp.maximum(top_a, top_b)
    fade_a = jnp.exp(top_a - top)
    fade_b = jnp.exp(top_b - top)
    return (
        top,
        total_a * fade_a + total_b * fade_b,
        acc_a * fade_a[..., None] + acc_b * fade_b[..., None],
    )


def fold_sources(parts):
    tops, totals, accs = parts
    top = jnp.max(tops, axis=0)
    fade = jnp.exp(tops - top[None])
    return (top, jnp.sum(totals * fade, axis=0), jnp.sum(accs * fade[..., None], axis=0))


def per_device(
    tokens,
    lengths,
    latent_cache,
    rope_cache,
    gain_in,
    w_down_q,
    w_down_kv,
    w_rope_key,
    gain_q,
    w_up_qn,
    w_up_qr,
    gain_kv,
    w_key_up,
    w_value_up,
    w_attn_out,
    gain_mid,
    w_ff_in,
    w_ff_out,
):
    f32 = jnp.float32
    bf16 = jnp.bfloat16
    highest = lax.Precision.HIGHEST
    scale = (NOPE + ROPE) ** (-0.5)
    resid = tokens.astype(f32)
    scaled_in = (resid * gain_in.astype(f32)).astype(bf16)
    part_q = jnp.dot(scaled_in, w_down_q, preferred_element_type=f32)
    part_kv = jnp.dot(scaled_in, w_down_kv, preferred_element_type=f32)
    part_rope = jnp.dot(scaled_in, w_rope_key, preferred_element_type=f32)
    square_in = jnp.sum(resid * resid, axis=1)
    sum_q, sum_kv, sum_rope, total_in = lax.psum((part_q, part_kv, part_rope, square_in), "kv")
    inv_in = lax.rsqrt(total_in / D + EPS)[:, None]
    query_latent = rms_scaled(inv_in * sum_q, gain_q).astype(bf16)
    new_latent = rms_scaled(inv_in * sum_kv, gain_kv).astype(bf16)
    new_rope_key = rotate((inv_in * sum_rope)[:, None, :], lengths)[:, 0, :].astype(bf16)
    query_nope = jnp.einsum(
        "bc,chd->bhd", query_latent, w_up_qn, preferred_element_type=f32
    ).astype(bf16)
    query_rope = rotate(
        jnp.einsum("bc,chr->bhr", query_latent, w_up_qr, preferred_element_type=f32), lengths
    ).astype(bf16)
    query_cache = jnp.einsum(
        "bhd,khd->bhk", query_nope, w_key_up, preferred_element_type=f32
    ).astype(bf16)
    rows = latent_cache.shape[1]
    positions = lax.axis_index(("kv", "tp")) * rows + jnp.arange(rows, dtype=jnp.int32)
    live = (positions[None, :] < lengths[:, None])[:, None, :]
    scores = (
        jnp.einsum("bhk,blk->bhl", query_cache, latent_cache, preferred_element_type=f32)
        + jnp.einsum("bhr,blr->bhl", query_rope, rope_cache, preferred_element_type=f32)
    ) * scale
    scores = jnp.where(live, scores, -1e30)
    top = jnp.max(scores, axis=2)
    weights = jnp.where(live, jnp.exp(scores - top[:, :, None]), 0.0)
    total = jnp.sum(weights, axis=2)
    acc = jnp.einsum("bhl,blk->bhk", weights.astype(bf16), latent_cache, preferred_element_type=f32)
    heads_dev = w_attn_out.shape[0]
    first_head = lax.axis_index("tp") * heads_dev
    own_value_up = lax.dynamic_slice_in_dim(w_value_up, first_head, heads_dev, 1).astype(f32)
    own_cache_q = lax.dynamic_slice_in_dim(query_cache, first_head, heads_dev, 1)
    own_rope_q = lax.dynamic_slice_in_dim(query_rope, first_head, heads_dev, 1)
    self_score = (
        jnp.einsum("bhk,bk->bh", own_cache_q, new_latent, preferred_element_type=f32)
        + jnp.einsum("bhr,br->bh", own_rope_q, new_rope_key, preferred_element_type=f32)
    ) * scale
    top, total, acc = fold_sources(
        (
            lax.all_to_all(top[None], "tp", split_axis=2, concat_axis=0, tiled=True),
            lax.all_to_all(total[None], "tp", split_axis=2, concat_axis=0, tiled=True),
            lax.all_to_all(acc[None], "tp", split_axis=2, concat_axis=0, tiled=True),
        )
    )
    top, total, acc = combined_all((top, total, acc), "kv", combine)
    joined = jnp.maximum(top, self_score)
    fade = jnp.exp(top - joined)
    self_weight = jnp.exp(self_score - joined)
    total = total * fade + self_weight
    acc = (
        acc * fade[:, :, None]
        + self_weight.astype(bf16).astype(f32)[:, :, None] * new_latent.astype(f32)[:, None, :]
    )
    expanded = jnp.einsum("bhk,khv->bhv", acc, own_value_up, precision=highest)
    head_out = (expanded / total[:, :, None]).astype(bf16)
    attn_part = jnp.einsum("bhv,hvd->bd", head_out, w_attn_out, preferred_element_type=f32)
    resid_mid = resid + lax.psum(attn_part, "tp")
    scaled_mid = (resid_mid * gain_mid.astype(f32)).astype(bf16)
    hidden_part = jnp.dot(scaled_mid, w_ff_in, preferred_element_type=f32)
    square_mid = jnp.sum(resid_mid * resid_mid, axis=1)
    hidden_sum, total_mid = lax.psum((hidden_part, square_mid), "kv")
    inv_mid = lax.rsqrt(total_mid / D + EPS)[:, None]
    hidden = jnp.square(jax.nn.relu(inv_mid * hidden_sum)).astype(bf16)
    out_part = jnp.dot(hidden, w_ff_out, preferred_element_type=f32)
    mixed = (resid_mid + lax.psum(out_part, "tp")).astype(bf16)
    return (mixed, new_latent, new_rope_key)


def solution(mesh):
    return jax.shard_map(
        per_device,
        mesh=mesh,
        in_specs=(
            P(None, "kv"),
            P(),
            P(None, ("kv", "tp"), None),
            P(None, ("kv", "tp"), None),
            P("kv"),
            P("kv", None),
            P("kv", None),
            P("kv", None),
            P(),
            P(),
            P(),
            P(),
            P(),
            P(),
            P("tp", None, "kv"),
            P("kv"),
            P("kv", "tp"),
            P("tp", "kv"),
        ),
        out_specs=(P(None, "kv"), P(), P()),
        check_vma=False,
    )
```

profile of v0, /device:TPU:0, one launch (start us, length us, event | category | flops | bytes accessed | tf_op | source)
XLA Modules:
  0.0 218.2 jit_solution(16655276583001931939)
XLA Ops:
  7.2 0.8 convert_element_type.75
  8.0 0.8 fusion.23
  8.8 0.7 convert_element_type.68
  9.5 0.7 broadcast_compare_fusion
  10.2 0.7 convert_element_type.70
  10.9 0.9 fusion.41
  11.7 1.1 fusion.43
  12.8 1.2 fusion.45
  14.0 30.8 %all-reduce = (f32[16,512]{1,0:T(8,128)S(1)}, f32[16]{0:T(128)S(1)}, f32[16,256]{1,0:T(8,128)S(1)}, f32[16,32]{1,0:T(8,128)S(1)}) all-reduce(f32[16,512]{1,0:T(8,128)S(1)} %fusion.45, f32[16]{0:T(128)S(1)} %fusion.23, f32[16,256]{1,0:T(8,128)S(1)} %fusion.43, f32[16,32]{1,0:T(8,128)S(1)} %fusion.41), channel_id=1, replica_groups=mesh['kv'=8,'tp'=4] {'kv'}, use_global_device_ids=true, to_apply=%region_2.0 | all-reduce | flops 12816 | bytes 102528 | tf_op jit(solution)/shard_map/psum | solution.py:96
  44.8 0.2 multiply_reduce_fusion.1
  45.0 0.1 multiply_cosine_fusion.1
  45.1 0.5 fusion.55
  45.6 0.7 convolution_convert_fusion
  46.3 0.1 subtract_convert_fusion
  46.4 0.1 pad_maximum_fusion
  46.5 0.1 fusion.14
  46.7 0.8 copy-done.1
  47.4 0.4 fusion.62
  47.8 0.7 copy.50
  48.5 3.7 %all-to-all-start = ((f32[1,16,16]{1,0,2:T(1,128)}), f32[1,16,16]{1,0,2:T(1,128)S(1)}, u32[]{:S(2)}, u32[]{:S(2)}) async-start(f32[1,16,16]{1,0,2:T(1,128)} %copy.50), calls=%async_computation | async-start | bytes 16384 | tf_op jit(solution)/shard_map/all_to_all | solution.py:133
  52.2 0.1 fusion.26
  52.3 0.6 copy-done.10
  53.0 0.1 fusion.35
  53.1 0.2 multiply_reduce_fusion.3
  53.3 0.3 convolution_bitcast_fusion
  53.6 0.7 fusion.52
  54.3 0.1 fusion.21
  54.5 0.5 copy-done.9
  54.9 0.1 fusion.27
  55.0 0.2 fusion.10
  55.3 0.6 copy-done.11
  56.1 0.7 copy.51
  56.8 0.8 copy.52
  57.6 4.2 %all-to-all-start.1 = ((f32[1,16,16]{1,0,2:T(1,128)}), f32[1,16,16]{1,0,2:T(1,128)S(1)}, u32[]{:S(2)}, u32[]{:S(2)}) async-start(f32[1,16,16]{1,0,2:T(1,128)} %copy.51), calls=%async_computation.1 | async-start | bytes 16384 | tf_op jit(solution)/shard_map/all_to_all | solution.py:134
  61.8 12.8 %all-gather.3 = f32[8,16,4]{1,2,0:T(4,128)S(1)} all-gather(f32[1,16,4]{1,2,0:T(4,128)S(1)} %bitcast.113), channel_id=2, replica_groups=mesh['kv'=8,'tp'=4] {'kv'}, dimensions={0}, use_global_device_ids=true | all-gather | bytes 2304 | tf_op jit(solution)/shard_map/all_gather | solution.py:13
  74.6 4.2 %all-to-all-start.2 = ((f32[1,16,16,256]{3,1,0,2:T(8,128)}), f32[1,16,16,256]{3,1,0,2:T(8,128)S(1)}, u32[]{:S(2)}, u32[]{:S(2)}) async-start(f32[1,16,16,256]{3,1,0,2:T(8,128)} %copy.52), calls=%async_computation.2 | async-start | bytes 524288 | tf_op jit(solution)/shard_map/all_to_all | solution.py:135
  78.8 12.8 %all-gather.4 = f32[8,16,4]{1,2,0:T(4,128)S(1)} all-gather(f32[1,16,4]{1,2,0:T(4,128)S(1)} %bitcast.114), channel_id=3, replica_groups=mesh['kv'=8,'tp'=4] {'kv'}, dimensions={0}, use_global_device_ids=true | all-gather | bytes 2304 | tf_op jit(solution)/shard_map/all_gather | solution.py:13
  91.6 0.1 multiply_reduce_fusion
  91.8 15.1 %all-gather.2 = f32[128,4,256]{2,1,0:T(4,128)S(1)} all-gather(f32[16,4,256]{2,1,0:T(4,128)S(1)} %copy.53), channel_id=4, replica_groups=mesh['kv'=8,'tp'=4] {'kv'}, dimensions={0}, use_global_device_ids=true | all-gather | bytes 589824 | tf_op jit(solution)/shard_map/all_gather | solution.py:13
  106.8 2.5 %while.19 = (s32[]{:T(128)}, f32[16,4]{0,1:T(4,128)S(1)}, f32[16,4]{0,1:T(4,128)S(1)}, f32[16,4,256]{2,1,0:T(4,128)S(1)}, f32[8,16,4]{1,2,0:T(4,128)S(1)}, /*ind...) while((s32[]{:T(128)}, f32[16,4]{0,1:T(4,128)S(1)}, ...), condition=%wide.region_10.11_spmd, body=%wide.region_9.10_spmd.sunk | while | flops 49541 | bytes 200335 | solution.py:18
  106.9 0.1 copy.81
  107.0 0.1 copy.82
  107.0 0.1 fusion.79
  107.4 0.1 fusion.79
  107.8 0.1 fusion.79
  107.9 0.1 copy.81
  108.0 0.1 copy.82
  108.1 0.1 fusion.79
  108.3 0.1 copy.81
  108.5 0.1 fusion.79
  108.8 0.1 fusion.79
  109.2 0.1 fusion.79
  109.4 0.1 copy.54
  109.5 0.1 multiply_add_fusion
  109.6 1.2 fusion.6
  110.8 0.2 convolution_bitcast_fusion.2
  111.0 16.5 %psum.60 = f32[16,256]{1,0:T(8,128)S(1)} all-reduce(f32[16,256]{1,0:T(8,128)S(1)} %convolution_bitcast_fusion.2), channel_id=1, replica_groups=mesh['kv'=8,'tp'=4] {'tp'}, use_global_device_ids=true, to_apply=%region_14.15 | all-reduce | flops 4096 | bytes 32768 | tf_op jit(solution)/shard_map/psum | solution.py:150
  127.5 0.1 multiply_reduce_fusion.2
  127.6 13.6 %psum.61 = f32[16]{0:T(128)S(1)} all-reduce(f32[16]{0:T(128)S(1)} %multiply_reduce_fusion.2), channel_id=1, replica_groups=mesh['kv'=8,'tp'=4] {'kv'}, use_global_device_ids=true, to_apply=%region_16.17 | all-reduce | flops 16 | bytes 128 | tf_op jit(solution)/shard_map/psum | solution.py:154
  141.2 0.9 fusion.38
  142.2 51.4 %all-reduce.3.cloned.1.call-done = f32[16,2048]{1,0:T(8,128)} async-done(((f32[16,2048]{1,0:T(8,128)}), f32[16,2048]{1,0:T(8,128)}) %all-reduce.3.cloned.1.call-update) | async-done | bytes 131088 | tf_op jit(solution)/shard_map/psum | solution.py:154
  193.6 1.2 fusion.12
  194.8 16.0 %psum.63 = f32[16,256]{1,0:T(8,128)S(1)} all-reduce(f32[16,256]{1,0:T(8,128)S(1)} %fusion.12), channel_id=1, replica_groups=mesh['kv'=8,'tp'=4] {'tp'}, use_global_device_ids=true, to_apply=%region_18.19 | all-reduce | flops 4096 | bytes 32768 | tf_op jit(solution)/shard_map/psum | solution.py:158
  210.7 0.6 add_convert_fusion.1
  (62 shorter events, 1.6 us)
Async XLA Ops:
  7.2 38.4 %copy-start = (bf16[512,16,64]{0,2,1:T(8,128)(2,1)S(1)}, bf16[512,16,64]{0,2,1:T(8,128)(2,1)}, u32[]{:S(2)}) copy-start(bf16[512,16,64]{0,2,1:T(8,128)(2,1)} %param.29) | copy-start | bytes 3145732
  7.2 37.9 %copy-start.4 = (bf16[512,16,32]{0,2,1:T(8,128)(2,1)S(1)}, bf16[512,16,32]{0,2,1:T(8,128)(2,1)}, u32[]{:S(2)}) copy-start(bf16[512,16,32]{0,2,1:T(8,128)(2,1)} %param.30) | copy-start | bytes 1572868
  12.8 32.8 %copy-start.5 = (bf16[256,16,64]{0,2,1:T(8,128)(2,1)S(1)}, bf16[256,16,64]{0,2,1:T(8,128)(2,1)}, u32[]{:S(2)}) copy-start(bf16[256,16,64]{0,2,1:T(8,128)(2,1)} %param.32) | copy-start | bytes 1572868
  45.6 0.9 copy-start.8
  46.3 1.2 copy-start.1
  48.5 9.1 %all-to-all-start = ((f32[1,16,16]{1,0,2:T(1,128)}), f32[1,16,16]{1,0,2:T(1,128)S(1)}, u32[]{:S(2)}, u32[]{:S(2)}) async-start(f32[1,16,16]{1,0,2:T(1,128)} %copy.50), calls=%async_computation | async-start | bytes 16384 | tf_op jit(solution)/shard_map/all_to_all | solution.py:133
  52.2 0.7 copy-start.10
  54.3 0.6 copy-start.9
  55.3 0.7 copy-start.11
  57.6 17.0 %all-to-all-start.1 = ((f32[1,16,16]{1,0,2:T(1,128)}), f32[1,16,16]{1,0,2:T(1,128)S(1)}, u32[]{:S(2)}, u32[]{:S(2)}) async-start(f32[1,16,16]{1,0,2:T(1,128)} %copy.51), calls=%async_computation.1 | async-start | bytes 16384 | tf_op jit(solution)/shard_map/all_to_all | solution.py:134
  74.6 17.0 %all-to-all-start.2 = ((f32[1,16,16,256]{3,1,0,2:T(8,128)}), f32[1,16,16,256]{3,1,0,2:T(8,128)S(1)}, u32[]{:S(2)}, u32[]{:S(2)}) async-start(f32[1,16,16,256]{3,1,0,2:T(8,128)} %copy.52), calls=%async_computation.2 | async-start | bytes 524288 | tf_op jit(solution)/shard_map/all_to_all | solution.py:135
  78.8 114.8 %all-reduce.3.cloned.1.call-start = ((), (), s32[]{:S(2)}) async-start(), calls=%async_computation.3 | async-start | bytes 262144 | tf_op jit(solution)/shard_map/psum | solution.py:154
  91.7 19.0 %copy-start.7 = (bf16[4,64,256]{2,1,0:T(8,128)(2,1)S(1)}, bf16[4,64,256]{2,1,0:T(8,128)(2,1)}, u32[]{:S(2)}) copy-start(bf16[4,64,256]{2,1,0:T(8,128)(2,1)} %param.34) | copy-start | bytes 393220
  106.8 34.4 %copy-start.2 = (bf16[256,2048]{1,0:T(8,128)(2,1)S(1)}, bf16[256,2048]{1,0:T(8,128)(2,1)}, u32[]{:S(2)}) copy-start(bf16[256,2048]{1,0:T(8,128)(2,1)} %param.36) | copy-start | bytes 3145732
  106.8 20.7 %copy-start.6 = (bf16[16,256]{1,0:T(8,128)(2,1)S(1)}, bf16[16,256]{1,0:T(8,128)(2,1)}, u32[]{:S(2)}) copy-start(bf16[16,256]{1,0:T(8,128)(2,1)} %param.20) | copy-start | bytes 24580
  109.3 84.3 %copy-start.3 = (bf16[2048,256]{1,0:T(8,128)(2,1)S(1)}, bf16[2048,256]{1,0:T(8,128)(2,1)}, u32[]{:S(2)}) copy-start(bf16[2048,256]{1,0:T(8,128)(2,1)} %param.37) | copy-start | bytes 3145732
Sparse Core Ops, SparseCore 0:
  142.3 51.2 all-reduce.2
where the time goes:
time: 219 us; the launch traced here: 218 us
  blocking collectives  117 us (53%)
  waiting for transfers between devices  51.5 us (24%)
  between operations  14.2 us (6%)
  starting transfers between devices  12.1 us (6%)
  matrix products  8.74 us (4%)
  other arithmetic  7.81 us (4%)
  local copies, waits for them, and re-layouts  6.26 us (3%)
    psum x1, waiting for transfers between devices, per_device(): hidden_sum, total_mid = lax.psum((hidden_part, square_mid), 'kv')  51.4 us
    all_gather x3, blocking collectives, combined_all(): gathered = jax.tree.map(lambda a: lax.all_gather(a, axis), part)  40.6 us
    psum x1, blocking collectives, per_device(): lax.psum((part_q, part_kv, part_rope, square_in), 'kv')  30.8 us
    psum x1, blocking collectives, per_device(): resid_mid = resid + lax.psum(attn_part, 'tp')  16.5 us
    psum x1, blocking collectives, per_device(): mixed = (resid_mid + lax.psum(out_part, 'tp')).astype(bf16)  16 us
    psum x1, blocking collectives, per_device(): hidden_sum, total_mid = lax.psum((hidden_part, square_mid), 'kv')  13.6 us
  transfers between devices with their start and end apart: 4, of which 1 were waited for; matrix products, arithmetic and copies ran while one was open for 2% of the time, Pallas kernels for 0%

commit v1 on v0

--- a/solution.py
+++ b/solution.py
@@ -7,6 +7,10 @@
 NOPE = 64
 ROPE = 32
 EPS = 1e-06
+
+
+def change_digits(s0):
+    return lax.all_gather(s0, axis_name="tp").sum(axis=0)
 
 
 def combined_all(part, axis, combine):
@@ -147,7 +151,7 @@
     expanded = jnp.einsum("bhk,khv->bhv", acc, own_value_up, precision=highest)
     head_out = (expanded / total[:, :, None]).astype(bf16)
     attn_part = jnp.einsum("bhv,hvd->bd", head_out, w_attn_out, preferred_element_type=f32)
-    resid_mid = resid + lax.psum(attn_part, "tp")
+    resid_mid = resid + change_digits(attn_part)
     scaled_mid = (resid_mid * gain_mid.astype(f32)).astype(bf16)
     hidden_part = jnp.dot(scaled_mid, w_ff_in, preferred_element_type=f32)
     square_mid = jnp.sum(resid_mid * resid_mid, axis=1)

time: 219 us -> 212 us (0.968)
  blocking collectives: 117 us -> 110 us
    psum x1 -> x0, blocking collectives: 16.5 us -> none  [per_device(): resid_mid = resid + lax.psum(attn_part, 'tp')]
    all_gather x0 -> x1, blocking collectives: none -> 8.75 us  [change_digits(): return lax.all_gather(s0, axis_name='tp').sum(axis=0)]
where the time goes in v1:
time: 212 us; the launch traced here: 211 us
  blocking collectives  110 us (52%)
  waiting for transfers between devices  52.4 us (25%)
  between operations  14.3 us (7%)
  starting transfers between devices  12.1 us (6%)
  matrix products  8.78 us (4%)
  other arithmetic  7.82 us (4%)
  local copies, waits for them, and re-layouts  6.25 us (3%)
    psum x1, waiting for transfers between devices, per_device(): hidden_sum, total_mid = lax.psum((hidden_part, square_mid), 'kv')  52.3 us
    all_gather x3, blocking collectives, combined_all(): gathered = jax.tree.map(lambda a: lax.all_gather(a, axis), part)  40.5 us
    psum x1, blocking collectives, per_device(): lax.psum((part_q, part_kv, part_rope, square_in), 'kv')  30.8 us
    psum x1, blocking collectives, per_device(): mixed = (resid_mid + lax.psum(out_part, 'tp')).astype(bf16)  16 us
    psum x1, blocking collectives, per_device(): hidden_sum, total_mid = lax.psum((hidden_part, square_mid), 'kv')  13.6 us
    all_gather x1, blocking collectives, change_digits(): return lax.all_gather(s0, axis_name='tp').sum(axis=0)  8.75 us
  transfers between devices with their start and end apart: 4, of which 1 were waited for; matrix products, arithmetic and copies ran while one was open for 2% of the time, Pallas kernels for 0%

profile of v1, /device:TPU:0, one launch (start us, length us, event | category | flops | bytes accessed | tf_op | source)
XLA Modules:
  0.0 211.3 jit_solution(5430203213944652060)
XLA Ops:
  7.2 0.8 convert_element_type.75
  8.0 0.8 fusion.23
  8.8 0.7 convert_element_type.68
  9.5 0.7 broadcast_compare_fusion
  10.2 0.7 convert_element_type.70
  10.9 0.9 fusion.41
  11.7 1.1 fusion.43
  12.8 1.2 fusion.45
  14.0 30.8 %all-reduce = (f32[16,512]{1,0:T(8,128)S(1)}, f32[16]{0:T(128)S(1)}, f32[16,256]{1,0:T(8,128)S(1)}, f32[16,32]{1,0:T(8,128)S(1)}) all-reduce(f32[16,512]{1,0:T(8,128)S(1)} %fusion.45, f32[16]{0:T(128)S(1)} %fusion.23, f32[16,256]{1,0:T(8,128)S(1)} %fusion.43, f32[16,32]{1,0:T(8,128)S(1)} %fusion.41), channel_id=1, replica_groups=mesh['kv'=8,'tp'=4] {'kv'}, use_global_device_ids=true, to_apply=%region_2.0 | all-reduce | flops 12816 | bytes 102528 | tf_op jit(solution)/shard_map/psum | solution.py:100
  44.8 0.2 multiply_reduce_fusion.1
  45.0 0.1 multiply_cosine_fusion.1
  45.1 0.5 fusion.55
  45.6 0.7 convolution_convert_fusion
  46.3 0.1 subtract_convert_fusion
  46.4 0.1 pad_maximum_fusion
  46.5 0.1 fusion.14
  46.7 0.8 copy-done.1
  47.4 0.4 fusion.62
  47.8 0.7 copy.50
  48.5 3.7 %all-to-all-start = ((f32[1,16,16]{1,0,2:T(1,128)}), f32[1,16,16]{1,0,2:T(1,128)S(1)}, u32[]{:S(2)}, u32[]{:S(2)}) async-start(f32[1,16,16]{1,0,2:T(1,128)} %copy.50), calls=%async_computation | async-start | bytes 16384 | tf_op jit(solution)/shard_map/all_to_all | solution.py:137
  52.2 0.1 fusion.26
  52.3 0.6 copy-done.10
  53.0 0.1 fusion.35
  53.1 0.2 multiply_reduce_fusion.3
  53.3 0.3 convolution_bitcast_fusion
  53.6 0.7 fusion.52
  54.3 0.1 fusion.21
  54.5 0.5 copy-done.9
  54.9 0.1 fusion.27
  55.0 0.2 fusion.10
  55.3 0.6 copy-done.11
  56.1 0.7 copy.51
  56.8 0.8 copy.52
  57.6 4.2 %all-to-all-start.1 = ((f32[1,16,16]{1,0,2:T(1,128)}), f32[1,16,16]{1,0,2:T(1,128)S(1)}, u32[]{:S(2)}, u32[]{:S(2)}) async-start(f32[1,16,16]{1,0,2:T(1,128)} %copy.51), calls=%async_computation.1 | async-start | bytes 16384 | tf_op jit(solution)/shard_map/all_to_all | solution.py:138
  61.8 12.8 %all-gather.4 = f32[8,16,4]{1,2,0:T(4,128)S(1)} all-gather(f32[1,16,4]{1,2,0:T(4,128)S(1)} %bitcast.115), channel_id=2, replica_groups=mesh['kv'=8,'tp'=4] {'kv'}, dimensions={0}, use_global_device_ids=true | all-gather | bytes 2304 | tf_op jit(solution)/shard_map/all_gather | solution.py:17
  74.6 4.2 %all-to-all-start.2 = ((f32[1,16,16,256]{3,1,0,2:T(8,128)}), f32[1,16,16,256]{3,1,0,2:T(8,128)S(1)}, u32[]{:S(2)}, u32[]{:S(2)}) async-start(f32[1,16,16,256]{3,1,0,2:T(8,128)} %copy.52), calls=%async_computation.2 | async-start | bytes 524288 | tf_op jit(solution)/shard_map/all_to_all | solution.py:139
  78.8 12.8 %all-gather.5 = f32[8,16,4]{1,2,0:T(4,128)S(1)} all-gather(f32[1,16,4]{1,2,0:T(4,128)S(1)} %bitcast.116), channel_id=3, replica_groups=mesh['kv'=8,'tp'=4] {'kv'}, dimensions={0}, use_global_device_ids=true | all-gather | bytes 2304 | tf_op jit(solution)/shard_map/all_gather | solution.py:17
  91.6 0.1 multiply_reduce_fusion
  91.7 14.9 %all-gather.2 = f32[128,4,256]{2,1,0:T(4,128)S(1)} all-gather(f32[16,4,256]{2,1,0:T(4,128)S(1)} %copy.53), channel_id=4, replica_groups=mesh['kv'=8,'tp'=4] {'kv'}, dimensions={0}, use_global_device_ids=true | all-gather | bytes 589824 | tf_op jit(solution)/shard_map/all_gather | solution.py:17
  106.7 2.5 %while.19 = (s32[]{:T(128)}, f32[16,4]{0,1:T(4,128)S(1)}, f32[16,4]{0,1:T(4,128)S(1)}, f32[16,4,256]{2,1,0:T(4,128)S(1)}, f32[8,16,4]{1,2,0:T(4,128)S(1)}, /*ind...) while((s32[]{:T(128)}, f32[16,4]{0,1:T(4,128)S(1)}, ...), condition=%wide.region_10.11_spmd, body=%wide.region_9.10_spmd.sunk | while | flops 49541 | bytes 200335 | solution.py:22
  106.7 0.1 copy.81
  106.8 0.1 copy.82
  106.9 0.1 fusion.79
  107.1 0.1 copy.81
  107.3 0.1 fusion.79
  107.6 0.1 fusion.79
  107.9 0.1 copy.82
  108.0 0.1 fusion.79
  108.2 0.1 copy.81
  108.3 0.1 fusion.79
  108.7 0.1 fusion.79
  109.0 0.1 fusion.79
  109.2 0.1 copy.54
  109.4 0.1 multiply_add_fusion
  109.5 1.2 fusion.6
  110.7 0.2 convolution_bitcast_fusion.2
  110.9 8.7 %all-gather.3 = f32[64,256]{1,0:T(8,128)S(1)} all-gather(f32[16,256]{1,0:T(8,128)S(1)} %convolution_bitcast_fusion.2), channel_id=5, replica_groups=mesh['kv'=8,'tp'=4] {'tp'}, dimensions={0}, use_global_device_ids=true | all-gather | bytes 81920 | tf_op jit(solution)/shard_map/all_gather | solution.py:13
  119.6 0.1 multiply_reduce_fusion.2
  119.8 13.6 %psum.53 = f32[16]{0:T(128)S(1)} all-reduce(f32[16]{0:T(128)S(1)} %multiply_reduce_fusion.2), channel_id=1, replica_groups=mesh['kv'=8,'tp'=4] {'kv'}, use_global_device_ids=true, to_apply=%region_16.17 | all-reduce | flops 16 | bytes 128 | tf_op jit(solution)/shard_map/psum | solution.py:158
  133.4 0.9 fusion.38
  134.3 52.3 %all-reduce.3.cloned.1.call-done = f32[16,2048]{1,0:T(8,128)} async-done(((f32[16,2048]{1,0:T(8,128)}), f32[16,2048]{1,0:T(8,128)}) %all-reduce.3.cloned.1.call-update) | async-done | bytes 131088 | tf_op jit(solution)/shard_map/psum | solution.py:158
  186.6 1.2 fusion.12
  187.8 16.0 %psum.55 = f32[16,256]{1,0:T(8,128)S(1)} all-reduce(f32[16,256]{1,0:T(8,128)S(1)} %fusion.12), channel_id=1, replica_groups=mesh['kv'=8,'tp'=4] {'tp'}, use_global_device_ids=true, to_apply=%region_18.19 | all-reduce | flops 4096 | bytes 32768 | tf_op jit(solution)/shard_map/psum | solution.py:162
  203.8 0.6 add_convert_fusion.1
  (63 shorter events, 1.6 us)
Async XLA Ops:
  7.2 38.4 %copy-start = (bf16[512,16,64]{0,2,1:T(8,128)(2,1)S(1)}, bf16[512,16,64]{0,2,1:T(8,128)(2,1)}, u32[]{:S(2)}) copy-start(bf16[512,16,64]{0,2,1:T(8,128)(2,1)} %param.29) | copy-start | bytes 3145732
  7.2 37.9 %copy-start.4 = (bf16[512,16,32]{0,2,1:T(8,128)(2,1)S(1)}, bf16[512,16,32]{0,2,1:T(8,128)(2,1)}, u32[]{:S(2)}) copy-start(bf16[512,16,32]{0,2,1:T(8,128)(2,1)} %param.30) | copy-start | bytes 1572868
  12.8 32.8 %copy-start.5 = (bf16[256,16,64]{0,2,1:T(8,128)(2,1)S(1)}, bf16[256,16,64]{0,2,1:T(8,128)(2,1)}, u32[]{:S(2)}) copy-start(bf16[256,16,64]{0,2,1:T(8,128)(2,1)} %param.32) | copy-start | bytes 1572868
  45.6 0.9 copy-start.8
  46.3 1.2 copy-start.1
  48.5 9.1 %all-to-all-start = ((f32[1,16,16]{1,0,2:T(1,128)}), f32[1,16,16]{1,0,2:T(1,128)S(1)}, u32[]{:S(2)}, u32[]{:S(2)}) async-start(f32[1,16,16]{1,0,2:T(1,128)} %copy.50), calls=%async_computation | async-start | bytes 16384 | tf_op jit(solution)/shard_map/all_to_all | solution.py:137
  52.2 0.7 copy-start.10
  54.3 0.6 copy-start.9
  55.3 0.7 copy-start.11
  57.6 17.0 %all-to-all-start.1 = ((f32[1,16,16]{1,0,2:T(1,128)}), f32[1,16,16]{1,0,2:T(1,128)S(1)}, u32[]{:S(2)}, u32[]{:S(2)}) async-start(f32[1,16,16]{1,0,2:T(1,128)} %copy.51), calls=%async_computation.1 | async-start | bytes 16384 | tf_op jit(solution)/shard_map/all_to_all | solution.py:138
  74.6 17.0 %all-to-all-start.2 = ((f32[1,16,16,256]{3,1,0,2:T(8,128)}), f32[1,16,16,256]{3,1,0,2:T(8,128)S(1)}, u32[]{:S(2)}, u32[]{:S(2)}) async-start(f32[1,16,16,256]{3,1,0,2:T(8,128)} %copy.52), calls=%async_computation.2 | async-start | bytes 524288 | tf_op jit(solution)/shard_map/all_to_all | solution.py:139
  78.8 107.8 %all-reduce.3.cloned.1.call-start = ((), (), s32[]{:S(2)}) async-start(), calls=%async_computation.3 | async-start | bytes 262144 | tf_op jit(solution)/shard_map/psum | solution.py:158
  106.7 4.0 %copy-start.7 = (bf16[4,64,256]{2,1,0:T(8,128)(2,1)S(1)}, bf16[4,64,256]{2,1,0:T(8,128)(2,1)}, u32[]{:S(2)}) copy-start(bf16[4,64,256]{2,1,0:T(8,128)(2,1)} %param.34) | copy-start | bytes 393220
  106.7 13.0 %copy-start.6 = (bf16[16,256]{1,0:T(8,128)(2,1)S(1)}, bf16[16,256]{1,0:T(8,128)(2,1)}, u32[]{:S(2)}) copy-start(bf16[16,256]{1,0:T(8,128)(2,1)} %param.20) | copy-start | bytes 24580
  106.7 26.7 %copy-start.2 = (bf16[256,2048]{1,0:T(8,128)(2,1)S(1)}, bf16[256,2048]{1,0:T(8,128)(2,1)}, u32[]{:S(2)}) copy-start(bf16[256,2048]{1,0:T(8,128)(2,1)} %param.36) | copy-start | bytes 3145732
  109.4 77.3 %copy-start.3 = (bf16[2048,256]{1,0:T(8,128)(2,1)S(1)}, bf16[2048,256]{1,0:T(8,128)(2,1)}, u32[]{:S(2)}) copy-start(bf16[2048,256]{1,0:T(8,128)(2,1)} %param.37) | copy-start | bytes 3145732
Sparse Core Ops, SparseCore 0:
  134.4 52.1 all-reduce.2
